TPU v7x, 32 devices: a whole 2x2x4 slice. The times are simulated.
32 devices in a mesh: sp: 4 (over z), tp: 4 (over y, x), dp: 2 (over core).
Axes of the slice: x: 2, y: 2, z: 4, core: 2. Of those that a mesh axis runs over, the one named last changes fastest.
Arguments:
- latents: bfloat16 [2, 1024, 4096], P('dp', ('sp', 'tp')), may hold values from -8 to 8
- cond: bfloat16 [2, 4096], P('dp', 'sp'), may hold values from -6 to 6
- cond_ctx: bfloat16 [4096], P('sp'), may hold values from -6 to 6
- context: bfloat16 [2, 1024, 4096], P('dp', 'sp'), may hold values from -8 to 8
- w_shift: bfloat16 [4096, 4096], P('sp', 'tp'), may hold values from -0.09375 to 0.09375
- w_scale: bfloat16 [4096, 4096], P('sp', 'tp'), may hold values from -0.09375 to 0.09375
- w_gate: bfloat16 [4096, 4096], P('sp', 'tp'), may hold values from -0.1875 to 0.1875
- gain_pre: bfloat16 [4096], replicated, may hold values from 0.099609375 to 1.8984375
- gain_post: bfloat16 [4096], replicated, may hold values from 0.099609375 to 1.8984375
- w_query: bfloat16 [4096, 1024], P('dp', 'tp'), may hold values from -0.09375 to 0.09375
- w_key: bfloat16 [4096, 1024], P('dp', 'tp'), may hold values from -0.09375 to 0.09375
- w_value: bfloat16 [4096, 2048], P('dp', 'tp'), may hold values from -0.09375 to 0.09375
- w_outgate: bfloat16 [4096, 2048], P('dp', 'tp'), may hold values from -0.09375 to 0.09375
- w_down: bfloat16 [4096, 32], replicated, may hold values from -0.25 to 0.25
- decay_up: bfloat16 [2, 16, 1024], P(None, None, 'tp'), may hold values from -1.5 to 1.5
- decay_bias: float32 [2, 1024], P(None, 'tp'), may hold values from -0.5 to 11
- head_gain: bfloat16 [2048], P('tp'), may hold values from 0.099609375 to 1.8984375
- w_out: bfloat16 [2048, 4096], P('tp', 'dp'), may hold values from -0.125 to 0.125
Outputs:
- mixer_out: bfloat16 [2, 1024, 4096], P('dp', ('sp', 'tp'))
All inputs are finite; a program needn't handle non-finite values.
Results may differ from a plain program's by a relative error of at most 0.015.
Values may be sent and summed in bfloat16 or wider, within the bound.
A program may use at most 128 MiB of HBM per device.

v0:
```python
import jax
import jax.numpy as jnp
from jax import lax
from jax.sharding import PartitionSpec as P

DK_HEAD = 256
DV_HEAD = 512
RANK = 16
BLOCK = 128


EPS = 1e-06
TAU = 16.0
HIGH_ACCURACY = lax.Precision.HIGHEST


def carried_in(value, axis, combine, identity, reverse):
    count, mine = (lax.axis_size(axis), lax.axis_index(axis))
    everything = jax.tree.map(lambda part: lax.all_gather(part, axis), value)
    start = jax.tree.map(
        lambda part, zero: jnp.broadcast_to(jnp.asarray(zero, part.dtype), part.shape),
        value,
        identity,
    )

    def hop(k, before):
        at = count - 1 - k if reverse else k
        reached = at > mine if reverse else at < mine
        new = combine(before, jax.tree.map(lambda part: part[at], everything))
        return jax.tree.map(lambda a, b: jnp.where(reached, a, b), new, before)

    return lax.fori_loop(0, count, hop, start)


def matmul(left, right):
    return jnp.dot(left, right, preferred_element_type=jnp.float32)


def rms_scale(vectors, gain):
    return vectors * lax.rsqrt(jnp.mean(vectors * vectors, axis=-1, keepdims=True) + EPS) * gain


def log_decays(lowrank, decay_up, decay_bias):
    result = []
    for direction in range(2):
        preact = (
            matmul(lowrank[:, direction * RANK : (direction + 1) * RANK], decay_up[direction])
            + decay_bias[direction]
        )
        result.append(jax.nn.log_sigmoid(preact) / TAU)
    return result


def chain(earlier, later):
    return (earlier[0] + later[0], earlier[1] * jnp.exp(later[0])[:, :, None] + later[1])


def reverse_rows(array):
    return jnp.flip(array, axis=1)


def local_pass(queries, keys_in, values, decays):
    heads_here, length, key_width = queries.shape
    count = length // BLOCK
    middle = BLOCK // 2

    def blocks(array):
        return jnp.moveaxis(array.reshape(heads_here, count, BLOCK, array.shape[-1]), 1, 0)

    causal = jnp.tril(jnp.ones((BLOCK, BLOCK), bool))

    def advance(carried_state, inputs):
        query_block_tile, key_block_tile, value_block_tile, block_g = inputs
        running_decay_sum = jnp.cumsum(block_g, axis=1)
        center = running_decay_sum[:, middle : middle + 1]
        scores = jnp.einsum(
            "htk,hsk->hts",
            query_block_tile * jnp.exp(running_decay_sum - center),
            key_block_tile * jnp.exp(center - running_decay_sum),
            precision=HIGH_ACCURACY,
        )
        scores = jnp.where(causal, scores, 0.0)
        final_state_value = running_decay_sum[:, -1:]
        output = jnp.einsum(
            "hts,hsv->htv", scores, value_block_tile, precision=HIGH_ACCURACY
        ) + jnp.einsum(
            "nyf,nfe->nye",
            query_block_tile * jnp.exp(running_decay_sum),
            carried_state,
            precision=HIGH_ACCURACY,
        )
        carried_state = carried_state * jnp.exp(final_state_value[:, 0])[:, :, None] + jnp.einsum(
            "dzg,dzu->dgu",
            key_block_tile * jnp.exp(final_state_value - running_decay_sum),
            value_block_tile,
            precision=HIGH_ACCURACY,
        )
        return (carried_state, output)

    initial = jnp.zeros((heads_here, key_width, values.shape[-1]), jnp.float32)
    carried_state, output = lax.scan(
        advance, initial, (blocks(queries), blocks(keys_in), blocks(values), blocks(decays))
    )
    output = jnp.moveaxis(output, 0, 1).reshape(heads_here, length, values.shape[-1])
    return (output, carried_state, jnp.sum(decays, axis=1))


def body(
    latents,
    cond,
    cond_ctx,
    context,
    w_shift,
    w_scale,
    w_gate,
    gain_pre,
    gain_post,
    w_query,
    w_key,
    w_value,
    w_outgate,
    w_down,
    decay_up,
    decay_bias,
    head_gain,
    w_out,
):
    width = gain_pre.shape[0]
    column_count = w_shift.shape[1]
    column_start = lax.axis_index("tp") * column_count
    activated = jax.nn.silu(cond.astype(jnp.float32)).astype(jnp.bfloat16)
    activated_ctx = jax.nn.silu(cond_ctx.astype(jnp.float32)).astype(jnp.bfloat16)[None, :]

    def placed(part):
        return lax.dynamic_update_slice_in_dim(
            jnp.zeros((part.shape[0], width), jnp.float32), part, column_start, 1
        )

    shift_vec, scale_vec, gate_vec, shift_ctx, scale_ctx = lax.psum(
        (
            placed(matmul(activated, w_shift)),
            placed(matmul(activated, w_scale)),
            placed(matmul(activated, w_gate)),
            placed(matmul(activated_ctx, w_shift)),
            placed(matmul(activated_ctx, w_scale)),
        ),
        ("sp", "tp"),
    )
    w_query, w_key, w_value, w_outgate, w_out = (
        lax.all_gather(w_query, "dp", axis=0, tiled=True),
        lax.all_gather(w_key, "dp", axis=0, tiled=True),
        lax.all_gather(w_value, "dp", axis=0, tiled=True),
        lax.all_gather(w_outgate, "dp", axis=0, tiled=True),
        lax.all_gather(w_out, "dp", axis=1, tiled=True),
    )

    def project(rows, mats):
        return tuple((matmul(rows, weight).astype(jnp.bfloat16) for weight in mats))

    gain_in = gain_pre.astype(jnp.float32)
    latent_rows = latents[0].astype(jnp.float32)
    modulated = (rms_scale(latent_rows, gain_in) * (1.0 + scale_vec[0]) + shift_vec[0]).astype(
        jnp.bfloat16
    )
    lowrank = matmul(modulated, w_down).astype(jnp.bfloat16)
    all_rows, all_lowrank = (
        lax.all_gather(modulated, "tp", axis=0, tiled=True),
        lax.all_gather(lowrank, "tp", axis=0, tiled=True),
    )
    queries, latent_keys, values, out_gate = project(all_rows, (w_query, w_key, w_value, w_outgate))
    decay_fwd, decay_bwd = log_decays(all_lowrank, decay_up, decay_bias)
    ctx_float = context[0].astype(jnp.float32)
    modulated_ctx = (rms_scale(ctx_float, gain_in) * (1.0 + scale_ctx[0]) + shift_ctx[0]).astype(
        jnp.bfloat16
    )
    keys_part, values_part = project(modulated_ctx, (w_key, w_value))
    ctx_keys, ctx_values, ctx_lowrank = (
        lax.all_gather(keys_part, "sp", axis=0, tiled=True),
        lax.all_gather(values_part, "sp", axis=0, tiled=True),
        lax.all_gather(
            matmul(modulated_ctx, w_down).astype(jnp.bfloat16), "sp", axis=0, tiled=True
        ),
    )
    heads_here = queries.shape[1] // DK_HEAD

    def by_head(array, head_width):
        return jnp.moveaxis(
            array.astype(jnp.float32).reshape(array.shape[0], heads_here, head_width), 1, 0
        )

    ctx_fwd, ctx_bwd = log_decays(ctx_lowrank, decay_up, decay_bias)
    ctx_head_keys = by_head(ctx_keys, DK_HEAD)
    ctx_head_values = by_head(ctx_values, DV_HEAD)
    ctx_head_fwd = by_head(ctx_fwd, DK_HEAD)
    ctx_head_bwd = by_head(ctx_bwd, DK_HEAD)
    ctx_cumulative = jnp.cumsum(ctx_head_fwd, axis=1)
    start_fwd = jnp.einsum(
        "dzg,dzu->dgu",
        ctx_head_keys * jnp.exp(ctx_cumulative[:, -1:] - ctx_cumulative),
        ctx_head_values,
        precision=HIGH_ACCURACY,
    )
    start_bwd = jnp.einsum(
        "dzg,dzu->dgu",
        ctx_head_keys * jnp.exp(jnp.cumsum(ctx_head_bwd, axis=1) - ctx_head_bwd),
        ctx_head_values,
        precision=HIGH_ACCURACY,
    )
    head_query_rows = by_head(queries, DK_HEAD) * DK_HEAD ** (-0.5)
    head_k = by_head(latent_keys, DK_HEAD)
    head_v = by_head(values, DV_HEAD)
    forward_head_output = by_head(decay_fwd, DK_HEAD)
    backward_head_output = reverse_rows(by_head(decay_bwd, DK_HEAD))
    out_fwd, state_fwd, total_fwd = local_pass(head_query_rows, head_k, head_v, forward_head_output)
    empty_pair = (jnp.zeros_like(total_fwd), jnp.zeros_like(state_fwd))
    prior_total, prior_state = carried_in((total_fwd, state_fwd), "sp", chain, empty_pair, False)
    forward_entry_state = start_fwd * jnp.exp(prior_total)[:, :, None] + prior_state
    out_fwd = out_fwd + jnp.einsum(
        "nyf,nfe->nye",
        head_query_rows * jnp.exp(jnp.cumsum(forward_head_output, axis=1)),
        forward_entry_state,
        precision=HIGH_ACCURACY,
    )
    reversed_query_rows = reverse_rows(head_query_rows)
    out_bwd, state_bwd, total_bwd = local_pass(
        reversed_query_rows, reverse_rows(head_k), reverse_rows(head_v), backward_head_output
    )
    later_total, later_state = carried_in((total_bwd, state_bwd), "sp", chain, empty_pair, True)
    backward_entry_state = start_bwd * jnp.exp(later_total)[:, :, None] + later_state
    out_bwd = out_bwd + jnp.einsum(
        "nyf,nfe->nye",
        reversed_query_rows * jnp.exp(jnp.cumsum(backward_head_output, axis=1)),
        backward_entry_state,
        precision=HIGH_ACCURACY,
    )
    mixed_sum = out_fwd + reverse_rows(out_bwd)
    gains_head = by_head(head_gain[None, :], DV_HEAD)
    gated_rows = rms_scale(mixed_sum, gains_head) * jax.nn.silu(by_head(out_gate, DV_HEAD))
    heads_out = (
        jnp.moveaxis(gated_rows, 0, 1)
        .reshape(gated_rows.shape[1], heads_here * DV_HEAD)
        .astype(jnp.bfloat16)
    )
    rounded = lax.optimization_barrier(matmul(heads_out, w_out).astype(jnp.bfloat16))
    projected = lax.psum_scatter(
        rounded.astype(jnp.float32).astype(jnp.bfloat16), "tp", scatter_dimension=0, tiled=True
    ).astype(jnp.float32)
    result_rows = latent_rows + gate_vec[0] * rms_scale(projected, gain_post.astype(jnp.float32))
    return result_rows.astype(jnp.bfloat16)[None]


def solution(mesh):
    return jax.shard_map(
        body,
        mesh=mesh,
        in_specs=(
            P("dp", ("sp", "tp"), None),
            P("dp", "sp"),
            P("sp"),
            P("dp", "sp", None),
            P("sp", "tp"),
            P("sp", "tp"),
            P("sp", "tp"),
            P(),
            P(),
            P("dp", "tp"),
            P("dp", "tp"),
            P("dp", "tp"),
            P("dp", "tp"),
            P(),
            P(None, None, "tp"),
            P(None, "tp"),
            P("tp"),
            P("tp", "dp"),
        ),
        out_specs=P("dp", ("sp", "tp"), None),
        check_vma=False,
    )
```

profile of v0, /device:TPU:0, one launch (start us, length us, event | category | flops | bytes accessed | tf_op | source)
XLA Modules:
  0.0 415.6 jit_solution(15403058340506022403)
XLA Ops:
  8.2 2.1 fusion.184
  14.4 109.8 %all-reduce.3.cloned.1.call-done = (f32[4096]{0:T(1024)}, f32[1,4096]{1,0:T(1,128)}, f32[4096]{0:T(1024)}, f32[1,4096]{1,0:T(1,128)}, f32[4096]{0:T(1024)}) async-done(((f32[4096]{0:T(1024)}, f32[1,4096]{1,0:T(1,128)}, f32[4096]{0:T(1024)}, f32[1,4096]{1,0:T(1,128)}, f32[4096]{0:T(1024)}), (f32[4096]{0:T(1024)}, f32[1,4096]{1,0:T(1,128)}, f32[4096]{0:T(1024)}, f32[1,4096]{1,0:T(1,128)}, ...) | async-done | bytes 81936 | tf_op jit(solution)/shard_map/psum | solution.py:139
  124.9 1.8 fusion.116
  128.4 8.2 %all-gather.4 = bf16[4,64,32]{1,2,0:T(8,128)(2,1)S(1)} all-gather(bf16[1,64,32]{1,2,0:T(8,128)(2,1)S(1)} %fusion.104), channel_id=1, replica_groups=mesh['sp'=4,'tp'=4,'dp'=2] {'tp'}, dimensions={0}, use_global_device_ids=true | all-gather | bytes 20480 | tf_op jit(solution)/shard_map/all_gather | solution.py:168
  137.1 24.8 %all-gather.17.cloned.1.call-done = bf16[256,4096]{1,0:T(8,128)(2,1)} async-done(((bf16[64,4096]{1,0:T(8,128)(2,1)}), bf16[256,4096]{1,0:T(8,128)(2,1)}) %all-gather.17.cloned.1.call-update) | async-done | bytes 2097168 | tf_op jit(solution)/shard_map/all_gather | solution.py:167
  161.8 2.9 fusion.103
  164.8 9.0 %all-gather.23.cloned.1.call-done = bf16[4096,256]{1,0:T(8,128)(2,1)} async-done(((bf16[2048,256]{1,0:T(8,128)(2,1)}), bf16[4096,256]{1,0:T(8,128)(2,1)}) %all-gather.23.cloned.1.call-update) | async-done | bytes 2097168 | tf_op jit(solution)/shard_map/all_gather | solution.py:150
  173.7 2.9 broadcast_multiply_fusion.2
  176.7 13.4 %all-gather.21.cloned.1.call-done = bf16[4096,512]{1,0:T(8,128)(2,1)} async-done(((bf16[2048,512]{1,0:T(8,128)(2,1)}), bf16[4096,512]{1,0:T(8,128)(2,1)}) %all-gather.21.cloned.1.call-update) | async-done | bytes 4194320 | tf_op jit(solution)/shard_map/all_gather | solution.py:152
  190.1 4.1 fusion.99
  194.2 4.2 %while.60 = (s32[]{:T(128)}, f32[1,256,512]{2,1,0:T(8,128)S(1)}, f32[2,1,128,512]{3,2,1,0:T(8,128)S(1)}, f32[2,1,128,256]{3,2,1,0:T(8,128)S(1)}, f32[2,1,128,256...) while((s32[]{:T(128)}, f32[1,256,512]{2,1,0:T(8,128)S(1)}, ...), condition=%wide.region_6.7_spmd.clone, body=%wide.region_4.6_spmd.clone.sunk | while | flops 558661632 | bytes 4600956 | solution.py:101
  201.6 4.2 %while.62 = (s32[]{:T(128)}, f32[1,256,512]{2,1,0:T(8,128)S(1)}, f32[2,1,128,512]{3,2,1,0:T(8,128)S(1)}, f32[2,1,128,256]{3,2,1,0:T(8,128)S(1)}, f32[2,1,128,256...) while((s32[]{:T(128)}, f32[1,256,512]{2,1,0:T(8,128)S(1)}, ...), condition=%wide.region_19.20_spmd.clone, body=%wide.region_17.19_spmd.clone.sunk | while | flops 558661632 | bytes 4600956 | solution.py:101
  206.8 2.4 fusion.84
  211.5 2.0 convolution_convert_fusion.2
  214.8 1.7 convolution_convert_fusion.7
  216.5 14.4 %all_gather.60 = bf16[1024,32]{0,1:T(8,128)(2,1)S(1)} all-gather(bf16[256,32]{0,1:T(8,128)(2,1)S(1)} %convolution_convert_fusion.7), channel_id=1, replica_groups=mesh['sp'=4,'tp'=4,'dp'=2] {'sp'}, dimensions={0}, use_global_device_ids=true | all-gather | bytes 81920 | tf_op jit(solution)/shard_map/all_gather | solution.py:180
  235.2 1.3 copy.69
  240.1 10.9 %all-gather.5 = f32[4,1,256]{2,1,0:T(1,128)S(1)} all-gather(f32[1,1,256]{2,1,0:T(1,128)S(1)} %bitcast.502), channel_id=2, replica_groups=mesh['sp'=4,'tp'=4,'dp'=2] {'sp'}, dimensions={0}, use_global_device_ids=true | all-gather | bytes 5120 | tf_op jit(solution)/shard_map/all_gather | solution.py:19
  251.0 7.6 %all-gather.6 = f32[4,1,256]{2,1,0:T(1,128)S(1)} all-gather(f32[1,1,256]{2,1,0:T(1,128)S(1)} %bitcast.498), channel_id=4, replica_groups=mesh['sp'=4,'tp'=4,'dp'=2] {'sp'}, dimensions={0}, use_global_device_ids=true | all-gather | bytes 5120 | tf_op jit(solution)/shard_map/all_gather | solution.py:19
  258.7 2.5 bitcast_add_fusion.2
  262.7 20.9 %all_gather.59 = bf16[1024,256]{1,0:T(8,128)(2,1)S(1)} all-gather(bf16[256,256]{1,0:T(8,128)(2,1)S(1)} %convolution_convert_fusion.4), channel_id=1, replica_groups=mesh['sp'=4,'tp'=4,'dp'=2] {'sp'}, dimensions={0}, use_global_device_ids=true | all-gather | bytes 655360 | tf_op jit(solution)/shard_map/all_gather | solution.py:178
  283.6 4.9 %while.61 = (s32[]{:T(128)}, f32[1,256]{1,0:T(1,128)S(1)}, f32[1,256,512]{2,1,0:T(8,128)S(1)}, s32[]{:T(128)}, f32[4,1,256]{2,1,0:T(1,128)S(1)}, /*index=5*/f32[4,1,256,512]{3,2,1,0:T(8,128)}, s32[]{:T(128)}, s32[]{:T(128)}) while((s32[]{:T(128)}, f32[1,256]{1,0:T(1,128)S(1)}, f32[1,256,512]{2,1,0:T(8,128)S(1)}, s32[]{:T(128)}, ...), condition=%wide.region_16.17_spmd.clone, body=%wide.region_15.16_spmd.clone.sunk | while | flops 525060 | bytes 1579127 | solution.py:32
  288.6 13.3 %all-gather.33.cloned.1.call-done = f32[4,256,512]{2,1,0:T(8,128)} async-done(((f32[1,256,512]{2,1,0:T(8,128)}), f32[4,256,512]{2,1,0:T(8,128)}) %all-gather.33.cloned.1.call-update) | async-done | bytes 2097168 | tf_op jit(solution)/shard_map/all_gather | solution.py:19
  301.9 5.0 %while.63 = (s32[]{:T(128)}, f32[1,256]{1,0:T(1,128)S(1)}, f32[1,256,512]{2,1,0:T(8,128)S(1)}, s32[]{:T(128)}, f32[4,1,256]{2,1,0:T(1,128)S(1)}, /*index=5*/f32[...) while((s32[]{:T(128)}, f32[1,256]{1,0:T(1,128)S(1)}, ...), condition=%wide.region_26.27_spmd.clone, body=%wide.region_25.26_spmd.clone.sunk | while | flops 525064 | bytes 1579189 | solution.py:32
  306.9 23.2 %all-gather.25.cloned.1.call-done = bf16[1024,512]{1,0:T(8,128)(2,1)} async-done(((bf16[256,512]{1,0:T(8,128)(2,1)}), bf16[1024,512]{1,0:T(8,128)(2,1)}) %all-gather.25.cloned.1.call-update) | async-done | bytes 1048592 | tf_op jit(solution)/shard_map/all_gather | solution.py:179
  330.1 2.7 fusion.97
  334.1 2.3 fusion.95
  337.2 7.4 %all-gather.27.cloned.1.call-done = bf16[4096,512]{1,0:T(8,128)(2,1)} async-done(((bf16[2048,512]{1,0:T(8,128)(2,1)}), bf16[4096,512]{1,0:T(8,128)(2,1)}) %all-gather.27.cloned.1.call-update) | async-done | bytes 4194320 | tf_op jit(solution)/shard_map/all_gather | solution.py:153
  344.6 16.3 %all-gather.29.cloned.1.call-done = bf16[512,4096]{1,0:T(8,128)(2,1)} async-done(((bf16[512,2048]{1,0:T(8,128)(2,1)}), bf16[512,4096]{1,0:T(8,128)(2,1)}) %all-gather.29.cloned.1.call-update) | async-done | bytes 4194320 | tf_op jit(solution)/shard_map/all_gather | solution.py:154
  360.9 7.3 %convolution_convert_fusion = bf16[256,4096]{1,0:T(8,128)(2,1)} fusion(bf16[512,4096]{1,0:T(8,128)(2,1)} %all-gather.29.cloned.1.call-done, bf16[256,4096]{1,0:T(8,128)(2,1)S(1)} %copy-done.6, bf16[4096,512]{1,0:T(8,128)(2,1)} %all-gather.27.cloned.1.call-done, f32[256,512]{1,0:T(8,128)S(1)} %get-tuple-element.582, f32[512]{0:T(512)S(1)} %convert_element_type.113, ...), kind=kOutput, calls=%fused_computation.102 | convolution fusion | flops 2149842944 | bytes 13110272 | tf_op jit(solution)/shard_map/dot_general | solution.py:36
  368.9 35.7 %reduce-scatter.2.cloned.1.call-done = bf16[64,4096]{1,0:T(8,128)(2,1)} async-done(((bf16[256,4096]{1,0:T(8,128)(2,1)}), bf16[64,4096]{1,0:T(8,128)(2,1)}) %reduce-scatter.2.cloned.1.call-update) | async-done | bytes 524304 | tf_op jit(solution)/shard_map/reduce_scatter | solution.py:245
  405.9 2.1 fusion.131
  (253 shorter events, 46.3 us)
Async XLA Ops:
  7.4 3.8 copy-start
  7.4 3.0 copy-start.36
  7.4 116.8 %all-reduce.3.cloned.1.call-start = ((), (), s32[]{:S(2)}) async-start(), calls=%async_computation.11 | async-start | bytes 163840 | tf_op jit(solution)/shard_map/psum | solution.py:139
  7.4 3.0 copy-start.5
  11.6 2.8 copy-start.41
  13.5 123.6 %all-gather.19.cloned.1.call-start = ((), (), s32[]{:S(2)}) async-start(), calls=%async_computation.2 | async-start | bytes 3145728 | tf_op jit(solution)/shard_map/all_gather | solution.py:151
  14.1 147.8 %all-gather.17.cloned.1.call-start = ((), (), s32[]{:S(2)}) async-start(), calls=%async_computation.1 | async-start | bytes 2621440 | tf_op jit(solution)/shard_map/all_gather | solution.py:167
  14.3 113.6 %copy-start.29 = (f32[4096]{0:T(1024)}, f32[4096]{0:T(1024)S(1)}, u32[]{:S(2)}) copy-start(f32[4096]{0:T(1024)S(1)} %convert_element_type.96) | copy-start | bytes 49156
  126.7 10.0 %copy-start.46 = (bf16[2,16,256]{2,1,0:T(8,128)(2,1)S(1)}, bf16[2,16,256]{2,1,0:T(8,128)(2,1)}, u32[]{:S(2)}) copy-start(bf16[2,16,256]{2,1,0:T(8,128)(2,1)} %param.40) | copy-start | bytes 49156
  126.7 47.1 %all-gather.23.cloned.1.call-start = ((), (), s32[]{:S(2)}) async-start(), calls=%async_computation.4 | async-start | bytes 3145728 | tf_op jit(solution)/shard_map/all_gather | solution.py:150
  127.3 62.8 %all-gather.21.cloned.1.call-start = ((), (), s32[]{:S(2)}) async-start(), calls=%async_computation.3 | async-start | bytes 6291456 | tf_op jit(solution)/shard_map/all_gather | solution.py:152
  128.0 155.6 %all-gather.31.cloned.1.call-start = ((), (), s32[]{:S(2)}) async-start(), calls=%async_computation.9 | async-start | bytes 2621440 | tf_op jit(solution)/shard_map/all_gather | solution.py:19
  136.6 28.1 %copy-start.39 = (bf16[256,32]{0,1:T(8,128)(2,1)}, bf16[256,32]{0,1:T(8,128)(2,1)S(1)}, u32[]{:S(2)}) copy-start(bf16[256,32]{0,1:T(8,128)(2,1)S(1)} %reshape.786) | copy-start | bytes 49156
  176.7 24.1 %copy-start.16 = (f32[256,256]{1,0:T(8,128)}, f32[256,256]{1,0:T(8,128)S(1)}, u32[]{:S(2)}) copy-start(f32[256,256]{1,0:T(8,128)S(1)} %get-tuple-element.578) | copy-start | bytes 786436
  198.4 2.8 copy-start.14
  199.2 102.6 %all-gather.33.cloned.1.call-start = ((), (), s32[]{:S(2)}) async-start(), calls=%async_computation.10 | async-start | bytes 2621440 | tf_op jit(solution)/shard_map/all_gather | solution.py:19
  205.8 3.5 copy-start.24
  205.8 3.5 copy-start.40
  205.8 3.5 copy-start.30
  205.8 3.5 copy-start.38
  206.6 123.5 %all-gather.25.cloned.1.call-start = ((), (), s32[]{:S(2)}) async-start(), calls=%async_computation.5 | async-start | bytes 1310720 | tf_op jit(solution)/shard_map/all_gather | solution.py:179
  213.6 131.0 %all-gather.27.cloned.1.call-start = ((), (), s32[]{:S(2)}) async-start(), calls=%async_computation.6 | async-start | bytes 6291456 | tf_op jit(solution)/shard_map/all_gather | solution.py:153
  214.1 16.7 %copy-start.47 = (bf16[2,16,256]{2,1,0:T(8,128)(2,1)S(1)}, bf16[2,16,256]{2,1,0:T(8,128)(2,1)}, u32[]{:S(2)}) copy-start(bf16[2,16,256]{2,1,0:T(8,128)(2,1)} %param.40) | copy-start | bytes 49156
  214.2 146.7 %all-gather.29.cloned.1.call-start = ((), (), s32[]{:S(2)}) async-start(), calls=%async_computation.7 | async-start | bytes 6291456 | tf_op jit(solution)/shard_map/all_gather | solution.py:154
  214.7 189.9 %reduce-scatter.2.cloned.1.call-start = ((), (), s32[]{:S(2)}) async-start(), calls=%async_computation.8 | async-start | bytes 2621440 | tf_op jit(solution)/shard_map/reduce_scatter | solution.py:245
  258.7 3.2 copy-start.27
  258.7 3.3 copy-start.23
  301.9 28.2 %copy-start.13 = (f32[1024,256]{1,0:T(8,128)S(1)}, f32[1024,256]{1,0:T(8,128)}, u32[]{:S(2)}) copy-start(f32[1024,256]{1,0:T(8,128)} %copy-done.12) | copy-start | bytes 3145732
  336.4 24.5 %copy-start.6 = (bf16[256,4096]{1,0:T(8,128)(2,1)S(1)}, bf16[256,4096]{1,0:T(8,128)(2,1)}, u32[]{:S(2)}) copy-start(bf16[256,4096]{1,0:T(8,128)(2,1)} %all-gather.17.cloned.1.call-done) | copy-start | bytes 6291460
  368.2 37.7 %copy-start.8 = (bf16[1,64,4096]{2,1,0:T(8,128)(2,1)S(1)}, bf16[1,64,4096]{2,1,0:T(8,128)(2,1)}, u32[]{:S(2)}) copy-start(bf16[1,64,4096]{2,1,0:T(8,128)(2,1)} %param.26) | copy-start | bytes 1572868
  368.2 37.7 %copy-start.37 = (f32[4096]{0:T(1024)S(1)}, f32[4096]{0:T(1024)}, u32[]{:S(2)}) copy-start(f32[4096]{0:T(1024)} %get-tuple-element.568) | copy-start | bytes 49156
  368.2 39.8 %copy-start.1 = (bf16[1024,1024]{1,0:T(8,128)(2,1)S(1)}, bf16[1024,1024]{1,0:T(8,128)(2,1)}, u32[]{:S(2)}) copy-start(bf16[1024,1024]{1,0:T(8,128)(2,1)} %param.31) | copy-start | bytes 6291460
  (27 other events, 43.5 us)
Sparse Core Ops, SparseCore 0:
  14.5 109.6 all-reduce.2
  199.4 47.9 all-gather.30
  248.9 52.8 all-gather.32
  303.3 26.7 all-gather.24
  331.5 13.0 all-gather.26
  346.0 14.8 all-gather.28
Sparse Core Ops, SparseCore 1:
  15.5 13.0 all-gather.18
  126.7 35.0 all-gather.16
  163.3 10.4 all-gather.22
  175.3 14.7 all-gather.20
  368.3 36.2 reduce-scatter.1
where the time goes:
time: 417 us; the launch traced here: 416 us
  waiting for transfers between devices  256 us (61%)
  blocking collectives  61.9 us (15%)
  matrix products  42.3 us (10%)
  other arithmetic  27.1 us (6%)
  between operations  16 us (4%)
  local copies, waits for them, and re-layouts  11.5 us (3%)
    psum x1, waiting for transfers between devices, body(): lax.psum((placed(matmul(activated, w_shift)), placed(matmul(activated, w_...  110 us
    reduce_scatter x1, waiting for transfers between devices, body(): lax.psum_scatter(rounded.astype(jnp.float32).astype(jnp.bfloat16), 'tp',...  35.7 us
    dot_general x17, matrix products, matmul(): return jnp.dot(left, right, preferred_element_type=jnp.float32)  28.7 us
    all_gather x1, waiting for transfers between devices, body(): lax.all_gather(modulated, 'tp', axis=0, tiled=True)  24.8 us
    all_gather x1, waiting for transfers between devices, body(): lax.all_gather(values_part, 'sp', axis=0, tiled=True)  23.2 us
    all_gather x1, blocking collectives, body(): lax.all_gather(keys_part, 'sp', axis=0, tiled=True)  20.9 us
    all_gather x2, blocking collectives, carried_in(): everything = jax.tree.map(lambda part: lax.all_gather(part, axis), value)  18.4 us
    all_gather x1, waiting for transfers between devices, body(): lax.all_gather(w_out, 'dp', axis=1, tiled=True)  16.3 us
  transfers between devices with their start and end apart: 11, of which 9 were waited for; matrix products, arithmetic and copies ran while one was open for 12% of the time, Pallas kernels for 0%

commit v1 on v0

v1 whole, which is shorter than its diff:
```python
import functools

import jax
import jax.numpy as jnp
from jax import lax
from jax.experimental import pallas as pl
from jax.experimental.pallas import tpu as pltpu
from jax.sharding import PartitionSpec as P

RANK = 16
EPS = 1e-06
TAU = 16.0
SUB = 64
CH = 4
MESH = pl.DeviceIdType.MESH
F32 = jnp.float32
BF16 = jnp.bfloat16


def dot(a, b, dims=((1,), (0,))):
    return lax.dot_general(a, b, (dims, ((), ())), preferred_element_type=F32)


def silu(v):
    return v / (1.0 + jnp.exp(-v))


def log_sigmoid(v):
    return jnp.minimum(v, 0.0) - jnp.log1p(jnp.exp(-jnp.abs(v)))


def tri_sum(tri, g):
    high = g.astype(BF16)
    low = (g - high.astype(F32)).astype(BF16)
    return dot(tri, high) + dot(tri, low)


def triangle(n, upper):
    row = lax.broadcasted_iota(jnp.int32, (n, n), 0)
    col = lax.broadcasted_iota(jnp.int32, (n, n), 1)
    keep = (col >= row) if upper else (col <= row)
    return jnp.where(keep, 1.0, 0.0).astype(BF16)


def kernel(
    n_sp, n_tp, n_dp,
    lat_ref, cond_ref, cctx_ref, ctx_ref, wsh_hbm, wsc_hbm, wga_hbm, gpre_ref, gpost_ref,
    wq_hbm, wk_hbm, wv_hbm, wg_hbm, wdown_ref, up_ref, bias_ref, hgain_ref, wout_hbm,
    out_ref,
    wsh, wsc, wga, wq, wk, wv, wg, wout,
    lat_all, rows_lat, rows_ctx, part, mod_sp, mod_full,
    qb, kb, vb, gb, cum_f, cum_b, intra, heads,
    kc, vc, st_a, st_b,
    ry, rz, rf, rb, sy, sz, sf, sb, ra_f, ra_b, sa_f, sa_b,
    rs_send, rs_recv,
    lc_sem, wsend, wrecv, lsend, lrecv, m1send, m1recv, m2send, m2recv,
    csend, crecv, asend, arecv, osend, orecv, own_sem,
):
    sp, tp, dp = lax.axis_index("sp"), lax.axis_index("tp"), lax.axis_index("dp")
    half = n_tp // 2
    ty, tx = tp // 2, tp % 2

    def to(k):
        return ((ty + k // 2) % half) * 2 + (tx + k % 2) % 2

    def source(k):
        return ((ty + half - k // 2) % half) * 2 + (tx + k % 2) % 2

    rows_own = lat_ref.shape[0]
    rows = rows_own * n_tp
    cb = part.shape[1]

    def remote(src, dst, s, r, dev):
        return pltpu.make_async_remote_copy(
            src_ref=src, dst_ref=dst, send_sem=s, recv_sem=r, device_id=dev, device_id_type=MESH
        )

    mod_copies = []
    for i, (a, b) in enumerate(((wsh_hbm, wsh), (wsc_hbm, wsc), (wga_hbm, wga))):
        c = pltpu.make_async_copy(a, b, lc_sem.at[i])
        c.start()
        mod_copies.append(c)
    own = pltpu.make_async_copy(lat_ref, lat_all.at[tp], own_sem.at[0])
    own.start()

    barrier = pltpu.get_barrier_semaphore()
    for k in range(1, n_tp):
        pl.semaphore_signal(barrier, inc=1, device_id={"tp": to(k)}, device_id_type=MESH)
    for k in range(1, n_sp):
        pl.semaphore_signal(
            barrier, inc=1, device_id={"sp": (sp + k) % n_sp}, device_id_type=MESH
        )
    for k in range(1, n_dp):
        pl.semaphore_signal(
            barrier, inc=1, device_id={"dp": (dp + k) % n_dp}, device_id_type=MESH
        )
    pl.semaphore_wait(barrier, n_tp + n_sp + n_dp - 3)

    hr = rows_own // 2
    lat_copies = {}

    def send_lat(k, h):
        c = remote(
            lat_ref.at[pl.ds(h * hr, hr)], lat_all.at[tp, pl.ds(h * hr, hr)],
            lsend.at[k - 1, h], lrecv.at[k - 1, h], {"tp": to(k)},
        )
        c.start()
        lat_copies[k, h] = c

    for k in range(1, n_tp - 1):
        send_lat(k, 0)

    weight_pairs = ((wk_hbm, wk), (wv_hbm, wv), (wq_hbm, wq), (wg_hbm, wg), (wout_hbm, wout))
    w_copies = []
    for i, (a, b) in enumerate(weight_pairs):
        c = pltpu.make_async_copy(a, b.at[dp], lc_sem.at[3 + i])
        c.start()
        group = [c]
        for k in range(1, n_dp):
            c = remote(a, b.at[dp], wsend.at[k - 1, i], wrecv.at[k - 1, i],
                       {"dp": (dp + k) % n_dp})
            c.start()
            group.append(c)
        w_copies.append(group)

    def weights_ready(i):
        w_copies[i][0].wait()
        for c in w_copies[i][1:]:
            c.wait_recv()

    shape = (16, cond_ref.shape[1])
    first = lax.broadcasted_iota(jnp.int32, shape, 0) == 0
    act = jnp.where(
        first,
        jnp.broadcast_to(silu(cond_ref[...].astype(F32)), shape),
        jnp.broadcast_to(silu(cctx_ref[...].astype(F32)), shape),
    ).astype(BF16)
    for c in mod_copies:
        c.wait()
    d_sh, d_sc, d_ga = dot(act, wsh[...]), dot(act, wsc[...]), dot(act, wga[...])
    part[...] = jnp.zeros_like(part)
    part[0:1] = d_sh[0:1]
    part[1:2] = d_sc[0:1]
    part[2:3] = d_ga[0:1]
    part[3:4] = d_sh[1:2]
    part[4:5] = d_sc[1:2]
    m1 = []
    for k in range(1, n_sp):
        c = remote(part, mod_sp.at[k - 1], m1send.at[k - 1], m1recv.at[k - 1],
                   {"sp": (sp + k) % n_sp})
        c.start()
        m1.append(c)
    total = part[...]
    for k, c in enumerate(m1):
        c.wait_recv()
        total = total + mod_sp[k]
    mod_full[tp] = total
    m2 = []
    for k in range(1, n_tp):
        c = remote(mod_full.at[tp], mod_full.at[tp], m2send.at[k - 1], m2recv.at[k - 1],
                   {"tp": to(k)})
        c.start()
        m2.append(c)
    for k in (n_tp - 1,):
        send_lat(k, 0)
        send_lat(k, 1)
    for k in range(1, n_tp - 1):
        send_lat(k, 1)
    for c in m2:
        c.wait_recv()

    def modulate(load, store, count, at):
        def step(r, carry):
            x = load(r * 16).astype(F32)
            inv = lax.rsqrt(jnp.mean(x * x, axis=-1, keepdims=True) + EPS)
            pieces = []
            for c in range(n_tp):
                gain = gpre_ref[:, c * cb : (c + 1) * cb].astype(F32)
                y = x[:, c * cb : (c + 1) * cb] * inv * gain
                y = y * (1.0 + mod_full[c, at + 1 : at + 2]) + mod_full[c, at : at + 1]
                pieces.append(y.astype(BF16))
            store(r * 16, jnp.concatenate(pieces, axis=1))
            return carry

        lax.fori_loop(0, count // 16, step, 0)

    def project(src, w):
        depth = w.shape[1]
        acc = dot(src[:, 0:depth], w[0])
        for d in range(1, n_dp):
            acc = acc + dot(src[:, d * depth : (d + 1) * depth], w[d])
        return acc.astype(BF16)

    def decays(src):
        low = dot(src[...], wdown_ref[...]).astype(BF16)
        return log_sigmoid(dot(low, up_ref[...]) + bias_ref[...]) * (1.0 / TAU)

    n_ctx = ctx_ref.shape[0]

    def store_ctx(r, val):
        rows_ctx[pl.ds(pl.multiple_of(r, 16), 16)] = val

    modulate(lambda r: ctx_ref[pl.ds(pl.multiple_of(r, 16), 16)], store_ctx, n_ctx, 3)
    weights_ready(0)
    weights_ready(1)
    dk = kb.shape[1]
    dv = vb.shape[1]
    kc[...] = project(rows_ctx, wk)
    vc[...] = project(rows_ctx, wv)
    g_ctx = decays(rows_ctx)
    cum = tri_sum(triangle(n_ctx, False), g_ctx)
    keys = kc[...].astype(F32)
    last = cum[n_ctx - 1 : n_ctx]
    key_f = (keys * jnp.exp(last[:, :dk] - cum[:, :dk])).astype(BF16)
    key_b = (keys * jnp.exp(cum[:, dk:] - g_ctx[:, dk:])).astype(BF16)
    st_a[...] = dot(vc[...], key_f, ((0,), (0,)))
    st_b[...] = dot(vc[...], key_b, ((0,), (0,)))
    tot_f = last[:, :dk]
    tot_b = last[:, dk:]

    up = {"sp": jnp.minimum(sp + 1, n_sp - 1)}
    down = {"sp": jnp.maximum(sp - 1, 0)}
    has_up = sp < n_sp - 1
    has_down = sp > 0
    cw = dv // CH

    def chunk(i):
        return pl.ds(i * cw, cw)

    def y_copy(i):
        return remote(sy.at[chunk(i)], ry.at[chunk(i)], csend.at[0, i], crecv.at[0, i], down)

    def z_copy(i):
        return remote(sz.at[chunk(i)], rz.at[chunk(i)], csend.at[1, i], crecv.at[1, i], up)

    def f_copy(i):
        return remote(sf.at[chunk(i)], rf.at[chunk(i)], csend.at[2, i], crecv.at[2, i], up)

    def b_copy(i):
        return remote(sb.at[chunk(i)], rb.at[chunk(i)], csend.at[3, i], crecv.at[3, i], down)

    a_f = remote(sa_f, ra_f, asend.at[0], arecv.at[0], down)
    a_b = remote(sa_b, ra_b, asend.at[1], arecv.at[1], up)

    @pl.when(jnp.logical_not(has_up))
    def _():
        ra_f[...] = jnp.zeros_like(ra_f)
        ry[...] = jnp.zeros_like(ry)

    @pl.when(jnp.logical_not(has_down))
    def _():
        ra_b[...] = jnp.zeros_like(ra_b)
        rz[...] = jnp.zeros_like(rz)

    @pl.when(has_up)
    def _():
        a_f.wait_recv()

    sa_f[...] = ra_f[...] + tot_f

    @pl.when(has_down)
    def _():
        a_f.start()
        a_b.wait_recv()

    sa_b[...] = ra_b[...] + tot_b

    @pl.when(has_up)
    def _():
        a_b.start()

    scale_f = jnp.exp(ra_f[0:1])
    scale_b = jnp.exp(ra_b[0:1])
    for i in range(CH):
        c = slice(i * cw, (i + 1) * cw)

        @pl.when(has_up)
        def _():
            y_copy(i).wait_recv()

        y = ry[c].astype(F32) + st_a[c] * scale_f
        sy[c] = y.astype(BF16)

        @pl.when(has_down)
        def _():
            y_copy(i).start()
            z_copy(i).wait_recv()

        z = rz[c].astype(F32) + st_b[c] * scale_b
        sz[c] = z.astype(BF16)

        @pl.when(has_up)
        def _():
            z_copy(i).start()

    @pl.when(jnp.logical_not(has_down))
    def _():
        rf[...] = sy[...]

    @pl.when(jnp.logical_not(has_up))
    def _():
        rb[...] = sz[...]

    def modulate_block(blk):
        def store(r, val):
            at = pl.multiple_of(blk * rows_own + r, 16)
            rows_lat[pl.ds(at, 16)] = val

        modulate(
            lambda r: lat_all[blk, pl.ds(pl.multiple_of(r, 16), 16)], store, rows_own, 0
        )

    own.wait()
    modulate_block(tp)
    for k in range(1, n_tp):
        lat_copies[k, 0].wait_recv()
        lat_copies[k, 1].wait_recv()
        modulate_block(source(k))

    kb[...] = project(rows_lat, wk)
    vb[...] = project(rows_lat, wv)
    g_lat = decays(rows_lat)
    cum_f[...] = tri_sum(triangle(rows, False), g_lat[:, :dk])
    cum_b[...] = tri_sum(triangle(rows, True), g_lat[:, dk:])
    keys = kb[...].astype(F32)
    end_f = cum_f[rows - 1 : rows]
    end_b = cum_b[0:1]
    key_f = (keys * jnp.exp(end_f - cum_f[...])).astype(BF16)
    key_b = (keys * jnp.exp(end_b - cum_b[...])).astype(BF16)
    st_a[...] = dot(vb[...], key_f, ((0,), (0,)))
    st_b[...] = dot(vb[...], key_b, ((0,), (0,)))
    step_f = jnp.exp(end_f)
    step_b = jnp.exp(end_b)

    def relay(i):
        c = slice(i * cw, (i + 1) * cw)

        @pl.when(has_down)
        def _():
            f_copy(i).wait_recv()

        sf[c] = (rf[c].astype(F32) * step_f + st_a[c]).astype(BF16)

        @pl.when(has_up)
        def _():
            f_copy(i).start()
            b_copy(i).wait_recv()

        sb[c] = (rb[c].astype(F32) * step_b + st_b[c]).astype(BF16)

        @pl.when(has_down)
        def _():
            b_copy(i).start()

    weights_ready(2)
    weights_ready(3)
    qb[...] = project(rows_lat, wq)
    gb[...] = project(rows_lat, wg)

    scale = dk ** -0.5
    n_sub = rows // SUB

    def block_scores(i):
        lo, hi, mid = i * SUB, (i + 1) * SUB, i * SUB + SUB // 2
        q = qb[lo:hi].astype(F32) * scale
        r_f = cum_f[mid : mid + 1]
        s_f = dot(
            (q * jnp.exp(cum_f[lo:hi] - r_f)).astype(BF16),
            (kb[0:hi].astype(F32) * jnp.exp(r_f - cum_f[0:hi])).astype(BF16),
            ((1,), (1,)),
        )
        t = lax.broadcasted_iota(jnp.int32, (SUB, hi), 0) + lo
        s = lax.broadcasted_iota(jnp.int32, (SUB, hi), 1)
        s_f = jnp.where(s <= t, s_f, 0.0)
        r_b = cum_b[mid : mid + 1]
        s_b = dot(
            (q * jnp.exp(cum_b[lo:hi] - r_b)).astype(BF16),
            (kb[lo:rows].astype(F32) * jnp.exp(r_b - cum_b[lo:rows])).astype(BF16),
            ((1,), (1,)),
        )
        t = lax.broadcasted_iota(jnp.int32, (SUB, rows - lo), 0)
        s = lax.broadcasted_iota(jnp.int32, (SUB, rows - lo), 1)
        s_b = jnp.where(s >= t, s_b, 0.0)
        intra[lo:hi] = dot(s_f.astype(BF16), vb[0:hi]) + dot(s_b.astype(BF16), vb[lo:rows])

    for i in range(CH):
        relay(i)
    for i in range(n_sub):
        block_scores(i)

    q = qb[...].astype(F32) * scale
    q_f = (q * jnp.exp(cum_f[...])).astype(BF16)
    q_b = (q * jnp.exp(cum_b[...])).astype(BF16)
    mixed = intra[...] + dot(q_f, rf[...], ((1,), (1,))) + dot(q_b, rb[...], ((1,), (1,)))
    inv = lax.rsqrt(jnp.mean(mixed * mixed, axis=-1, keepdims=True) + EPS)
    gated = mixed * inv * hgain_ref[...].astype(F32) * silu(gb[...].astype(F32))
    heads[...] = gated.astype(BF16)

    weights_ready(4)
    out_copies = []
    wc = wout.shape[2]
    for k in list(range(n_tp - 1, 0, -1)) + [0]:
        h = heads[pl.ds(pl.multiple_of(to(k) * rows_own, rows_own), rows_own)]
        for d in range(n_dp):
            rs_send[k, d] = dot(h, wout[d]).astype(BF16)
            if k:
                c = remote(rs_send.at[k, d], rs_recv.at[k - 1, d], osend.at[k - 1, d],
                           orecv.at[k - 1, d], {"tp": to(k)})
                c.start()
                out_copies.append(c)
    for c in out_copies:
        c.wait_recv()

    def finish(r, carry):
        at = pl.ds(pl.multiple_of(r * 16, 16), 16)
        proj = []
        for d in range(n_dp):
            v = rs_send[0, d, at].astype(F32)
            for k in range(1, n_tp):
                v = v + rs_recv[k - 1, d, at].astype(F32)
            proj.append(v)
        v = jnp.concatenate(proj, axis=1)
        inv = lax.rsqrt(jnp.mean(v * v, axis=-1, keepdims=True) + EPS)
        x = lat_ref[at].astype(F32)
        for c in range(n_tp):
            cols = slice(c * cb, (c + 1) * cb)
            y = v[:, cols] * inv * gpost_ref[:, cols].astype(F32)
            out_ref[at, cols] = (x[:, cols] + mod_full[c, 2:3] * y).astype(BF16)
        return carry

    lax.fori_loop(0, rows_own // 16, finish, 0)

    for c in out_copies + m1 + m2 + list(lat_copies.values()):
        c.wait_send()
    for group in w_copies:
        for c in group[1:]:
            c.wait_send()

    @pl.when(has_down)
    def _():
        a_f.wait_send()
        for i in range(CH):
            y_copy(i).wait_send()
            b_copy(i).wait_send()

    @pl.when(has_up)
    def _():
        a_b.wait_send()
        for i in range(CH):
            z_copy(i).wait_send()
            f_copy(i).wait_send()


def body(
    latents, cond, cond_ctx, context, w_shift, w_scale, w_gate, gain_pre, gain_post,
    w_query, w_key, w_value, w_outgate, w_down, decay_up, decay_bias, head_gain, w_out,
):
    n_sp, n_tp, n_dp = lax.axis_size("sp"), lax.axis_size("tp"), lax.axis_size("dp")
    width = gain_pre.shape[0]
    rows_own = latents.shape[1]
    rows = rows_own * n_tp
    n_ctx = context.shape[1]
    dk, dv = w_key.shape[1], w_value.shape[1]
    depth = w_key.shape[0]
    zero = jnp.zeros_like(decay_up[0])
    up = jnp.concatenate(
        [
            jnp.concatenate([decay_up[0], zero], axis=1),
            jnp.concatenate([zero, decay_up[1]], axis=1),
        ],
        axis=0,
    )
    mod_in, mod_cols = w_shift.shape
    vm = pl.BlockSpec(memory_space=pltpu.VMEM)
    hbm = pl.BlockSpec(memory_space=pl.ANY)
    V, D = pltpu.VMEM, pltpu.SemaphoreType.DMA
    scratch = [
        V((mod_in, mod_cols), BF16), V((mod_in, mod_cols), BF16), V((mod_in, mod_cols), BF16),
        V((n_dp, depth, dk), BF16), V((n_dp, depth, dk), BF16),
        V((n_dp, depth, dv), BF16), V((n_dp, depth, dv), BF16),
        V((n_dp,) + w_out.shape, BF16),
        V((n_tp, rows_own, width), BF16), V((rows, width), BF16), V((n_ctx, width), BF16),
        V((8, mod_cols), F32), V((max(n_sp - 1, 1), 8, mod_cols), F32),
        V((n_tp, 8, mod_cols), F32),
        V((rows, dk), BF16), V((rows, dk), BF16), V((rows, dv), BF16), V((rows, dv), BF16),
        V((rows, dk), F32), V((rows, dk), F32), V((rows, dv), F32), V((rows, dv), BF16),
        V((n_ctx, dk), BF16), V((n_ctx, dv), BF16), V((dv, dk), F32), V((dv, dk), F32),
    ]
    scratch += [V((dv, dk), BF16)] * 8
    scratch += [V((8, dk), F32)] * 4
    scratch += [
        V((n_tp,  n_dp, rows_own, w_out.shape[1]), BF16),
        V((n_tp - 1, n_dp, rows_own, w_out.shape[1]), BF16),
        D((8,)), D((n_dp - 1, 5)), D((n_dp - 1, 5)), D((n_tp - 1, 2)), D((n_tp - 1, 2)),
        D((n_sp - 1,)), D((n_sp - 1,)), D((n_tp - 1,)), D((n_tp - 1,)),
        D((4, CH)), D((4, CH)), D((2,)), D((2,)),
        D((n_tp - 1, n_dp)), D((n_tp - 1, n_dp)), D((1,)),
    ]
    out = pl.pallas_call(
        functools.partial(kernel, n_sp, n_tp, n_dp),
        out_shape=jax.ShapeDtypeStruct((rows_own, width), BF16),
        in_specs=[vm, vm, vm, vm, hbm, hbm, hbm, vm, vm, hbm, hbm, hbm, hbm, vm, vm, vm, vm, hbm],
        out_specs=vm,
        scratch_shapes=scratch,
        compiler_params=pltpu.CompilerParams(
            collective_id=0, has_side_effects=True, vmem_limit_bytes=60 * 1024 * 1024
        ),
    )(
        latents[0], cond, cond_ctx[None], context[0], w_shift, w_scale, w_gate,
        gain_pre[None], gain_post[None], w_query, w_key, w_value, w_outgate, w_down, up,
        decay_bias.reshape(1, -1), head_gain[None], w_out,
    )
    return out[None]


def solution(mesh):
    return jax.shard_map(
        body,
        mesh=mesh,
        in_specs=(
            P("dp", ("sp", "tp"), None),
            P("dp", "sp"),
            P("sp"),
            P("dp", "sp", None),
            P("sp", "tp"),
            P("sp", "tp"),
            P("sp", "tp"),
            P(),
            P(),
            P("dp", "tp"),
            P("dp", "tp"),
            P("dp", "tp"),
            P("dp", "tp"),
            P(),
            P(None, None, "tp"),
            P(None, "tp"),
            P("tp"),
            P("tp", "dp"),
        ),
        out_specs=P("dp", ("sp", "tp"), None),
        check_vma=False,
    )
```

time: 417 us -> 237 us (0.57)
  waiting for transfers between devices: 256 us -> 0 us
  Pallas kernels: 0 us -> 225 us
  blocking collectives: 61.9 us -> 0 us
  matrix products: 42.3 us -> 0 us
  other arithmetic: 27.1 us -> 0.62 us
  between operations: 16 us -> 0.01 us
    pallas_call x0 -> x1, Pallas kernels: none -> 225 us  [body(): pl.pallas_call(functools.partial(kernel, n_sp, n_tp, n_dp), out_shape=jax...]
    psum x1 -> x0, waiting for transfers between devices: 110 us -> none  [body(): lax.psum((placed(matmul(activated, w_shift)), placed(matmul(activated, w_...]
    all_gather x9 -> x0, waiting for transfers between devices: 107 us -> none  [the longest x1 24.8 us: body(): lax.all_gather(modulated, 'tp', axis=0, tiled=True)]
    all_gather x5 -> x0, blocking collectives: 61.9 us -> none  [the longest x1 20.9 us: body(): lax.all_gather(keys_part, 'sp', axis=0, tiled=True)]
    dot_general x37 -> x0, matrix products: 42.3 us -> none  [the longest x17 28.7 us: matmul(): return jnp.dot(left, right, preferred_element_type=jnp.float32)]
    reduce_scatter x1 -> x0, waiting for transfers between devices: 35.7 us -> none  [body(): lax.psum_scatter(rounded.astype(jnp.float32).astype(jnp.bfloat16), 'tp',...]
    select_n x16 -> x0, other arithmetic: 9.63 us -> none  [hop(): return jax.tree.map(lambda a, b: jnp.where(reached, a, b), new, before)]
    another operation x14 -> x0, other arithmetic: 6.39 us -> none
  transfers between devices with their start and end apart: 11 -> 0, of which waited for: 9 -> 0; matrix products, arithmetic and copies ran while one was open for 12% -> 0% of each run, Pallas kernels for 0% -> 0%
where the time goes in v1:
time: 237 us
  Pallas kernels  225 us (95%)
  local copies, waits for them, and re-layouts  11.3 us (5%)
    pallas_call x1, Pallas kernels, body(): pl.pallas_call(functools.partial(kernel, n_sp, n_tp, n_dp), out_shape=jax...  225 us
    unnamed x3, local copies, waits for them, and re-layouts  5.41 us

profile of v1, /device:TPU:0, one launch (start us, length us, event | category | flops | bytes accessed | tf_op | source)
XLA Modules:
  0.0 236.7 jit_solution(2062580091547918825)
XLA Ops:
  0.0 1.3 copy.20
  1.3 1.3 broadcast_in_dim.19.hgain_ref
  2.5 1.3 broadcast_in_dim.16.cctx_ref
  3.8 1.3 broadcast_in_dim.17.gpre_ref
  5.1 1.3 broadcast_in_dim.18.gpost_ref
  6.4 0.7 slice_bitcast_fusion.1
  7.1 0.6 fusion.2.up_ref
  7.8 2.3 copy.19.wdown_ref
  10.0 224.8 %shard_map.172 = bf16[64,4096]{1,0:T(8,128)(2,1)} custom-call(bf16[64,4096]{1,0:T(8,128)(2,1)} %bitcast.12, bf16[1,1024]{1,0:T(2,128)(2,1)} %cond_ref.1, bf16[1,1024]{1,0:T(2,128)(2,1)} %broadcast_in_dim.16.cctx_ref, bf16[256,4096]{1,0:T(8,128)(2,1)} %bitcast.10, bf16[1024,1024]{1,0:T(8,128)(2,1)} %wsh_hbm.1, bf16[1024,1024]{1,0:T(8,128)(2,1)} %wsc_hbm.1, ...), custom_call_target="tpu_custom_call" | custom-call | tf_op jit(solution)/shard_map/pallas_call | solution.py:499
  234.9 1.9 copy.22

commit v2 on v1

--- a/solution.py
+++ b/solution.py
@@ -44,9 +44,9 @@
 
 def kernel(
     n_sp, n_tp, n_dp,
-    lat_ref, cond_ref, cctx_ref, ctx_ref, wsh_hbm, wsc_hbm, wga_hbm, gpre_ref, gpost_ref,
-    wq_hbm, wk_hbm, wv_hbm, wg_hbm, wdown_ref, up_ref, bias_ref, hgain_ref, wout_hbm,
-    out_ref,
+    lat3, cond_ref, vec_ref, ctx3, wsh_hbm, wsc_hbm, wga_hbm,
+    wq_hbm, wk_hbm, wv_hbm, wg_hbm, wdown_ref, up_ref, bias_ref, wout_hbm,
+    out3,
     wsh, wsc, wga, wq, wk, wv, wg, wout,
     lat_all, rows_lat, rows_ctx, part, mod_sp, mod_full,
     qb, kb, vb, gb, cum_f, cum_b, intra, heads,
@@ -66,7 +66,13 @@
     def source(k):
         return ((ty + half - k // 2) % half) * 2 + (tx + k % 2) % 2
 
-    rows_own = lat_ref.shape[0]
+    lat_ref, ctx_ref, out_ref = lat3.at[0], ctx3.at[0], out3.at[0]
+    rows_own, width = lat_ref.shape
+    n_cond, n_head = cond_ref.shape[1], vb.shape[1]
+    gpre_ref = vec_ref.at[:, pl.ds(0, width)]
+    gpost_ref = vec_ref.at[:, pl.ds(width, width)]
+    cctx_ref = vec_ref.at[:, pl.ds(2 * width, n_cond)]
+    hgain_ref = vec_ref.at[:, pl.ds(2 * width + n_cond, n_head)]
     rows = rows_own * n_tp
     cb = part.shape[1]
 
@@ -192,8 +198,17 @@
         return acc.astype(BF16)
 
     def decays(src):
-        low = dot(src[...], wdown_ref[...]).astype(BF16)
-        return log_sigmoid(dot(low, up_ref[...]) + bias_ref[...]) * (1.0 / TAU)
+        low = dot(src[...], wdown_ref[...], ((1,), (1,))).astype(BF16)
+        zero = jnp.zeros_like(up_ref[0])
+        both = jnp.concatenate(
+            [
+                jnp.concatenate([up_ref[0], zero], axis=1),
+                jnp.concatenate([zero, up_ref[1]], axis=1),
+            ],
+            axis=0,
+        )
+        bias = jnp.concatenate([bias_ref[0:1], bias_ref[1:2]], axis=1)
+        return log_sigmoid(dot(low, both) + bias) * (1.0 / TAU)
 
     n_ctx = ctx_ref.shape[0]
 
@@ -252,55 +267,37 @@
         ra_b[...] = jnp.zeros_like(ra_b)
         rz[...] = jnp.zeros_like(rz)
 
-    @pl.when(has_up)
-    def _():
-        a_f.wait_recv()
-
-    sa_f[...] = ra_f[...] + tot_f
-
-    @pl.when(has_down)
-    def _():
-        a_f.start()
-        a_b.wait_recv()
-
-    sa_b[...] = ra_b[...] + tot_b
-
-    @pl.when(has_up)
-    def _():
-        a_b.start()
+    def a_down():
+        @pl.when(has_up)
+        def _():
+            a_f.wait_recv()
+
+        sa_f[...] = ra_f[...] + tot_f
+
+        @pl.when(has_down)
+        def _():
+            a_f.start()
+
+    def a_up():
+        @pl.when(has_down)
+        def _():
+            a_b.wait_recv()
+
+        sa_b[...] = ra_b[...] + tot_b
+
+        @pl.when(has_up)
+        def _():
+            a_b.start()
+
+    lower = 2 * sp < n_sp
+    upper = jnp.logical_not(lower)
+    pl.when(lower)(a_up)
+    pl.when(upper)(a_down)
+    pl.when(lower)(a_down)
+    pl.when(upper)(a_up)
 
     scale_f = jnp.exp(ra_f[0:1])
     scale_b = jnp.exp(ra_b[0:1])
-    for i in range(CH):
-        c = slice(i * cw, (i + 1) * cw)
-
-        @pl.when(has_up)
-        def _():
-            y_copy(i).wait_recv()
-
-        y = ry[c].astype(F32) + st_a[c] * scale_f
-        sy[c] = y.astype(BF16)
-
-        @pl.when(has_down)
-        def _():
-            y_copy(i).start()
-            z_copy(i).wait_recv()
-
-        z = rz[c].astype(F32) + st_b[c] * scale_b
-        sz[c] = z.astype(BF16)
-
-        @pl.when(has_up)
-        def _():
-            z_copy(i).start()
-
-    @pl.when(jnp.logical_not(has_down))
-    def _():
-        rf[...] = sy[...]
-
-    @pl.when(jnp.logical_not(has_up))
-    def _():
-        rb[...] = sz[...]
-
     def modulate_block(blk):
         def store(r, val):
             at = pl.multiple_of(blk * rows_own + r, 16)
@@ -310,8 +307,49 @@
             lambda r: lat_all[blk, pl.ds(pl.multiple_of(r, 16), 16)], store, rows_own, 0
         )
 
+    def y_pass():
+        for i in range(CH):
+            c = slice(i * cw, (i + 1) * cw)
+
+            @pl.when(has_up)
+            def _():
+                y_copy(i).wait_recv()
+
+            sy[c] = (ry[c].astype(F32) + st_a[c] * scale_f).astype(BF16)
+
+            @pl.when(has_down)
+            def _():
+                y_copy(i).start()
+
+    def z_pass():
+        for i in range(CH):
+            c = slice(i * cw, (i + 1) * cw)
+
+            @pl.when(has_down)
+            def _():
+                z_copy(i).wait_recv()
+
+            sz[c] = (rz[c].astype(F32) + st_b[c] * scale_b).astype(BF16)
+
+            @pl.when(has_up)
+            def _():
+                z_copy(i).start()
+
+    pl.when(lower)(z_pass)
+    pl.when(upper)(y_pass)
     own.wait()
     modulate_block(tp)
+    pl.when(lower)(y_pass)
+    pl.when(upper)(z_pass)
+
+    @pl.when(jnp.logical_not(has_down))
+    def _():
+        rf[...] = sy[...]
+
+    @pl.when(jnp.logical_not(has_up))
+    def _():
+        rb[...] = sz[...]
+
     for k in range(1, n_tp):
         lat_copies[k, 0].wait_recv()
         lat_copies[k, 1].wait_recv()
@@ -332,25 +370,34 @@
     step_f = jnp.exp(end_f)
     step_b = jnp.exp(end_b)
 
-    def relay(i):
-        c = slice(i * cw, (i + 1) * cw)
-
-        @pl.when(has_down)
-        def _():
-            f_copy(i).wait_recv()
-
-        sf[c] = (rf[c].astype(F32) * step_f + st_a[c]).astype(BF16)
-
-        @pl.when(has_up)
-        def _():
-            f_copy(i).start()
-            b_copy(i).wait_recv()
-
-        sb[c] = (rb[c].astype(F32) * step_b + st_b[c]).astype(BF16)
-
-        @pl.when(has_down)
-        def _():
-            b_copy(i).start()
+    def f_pass():
+        for i in range(CH):
+            c = slice(i * cw, (i + 1) * cw)
+
+            @pl.when(has_down)
+            def _():
+                f_copy(i).wait_recv()
+
+            @pl.when(has_up)
+            def _():
+                sf[c] = (rf[c].astype(F32) * step_f + st_a[c]).astype(BF16)
+                f_copy(i).start()
+
+    def b_pass():
+        for i in range(CH):
+            c = slice(i * cw, (i + 1) * cw)
+
+            @pl.when(has_up)
+            def _():
+                b_copy(i).wait_recv()
+
+            @pl.when(has_down)
+            def _():
+                sb[c] = (rb[c].astype(F32) * step_b + st_b[c]).astype(BF16)
+                b_copy(i).start()
+
+    pl.when(lower)(f_pass)
+    pl.when(upper)(b_pass)
 
     weights_ready(2)
     weights_ready(3)
@@ -383,10 +430,10 @@
         s_b = jnp.where(s >= t, s_b, 0.0)
         intra[lo:hi] = dot(s_f.astype(BF16), vb[0:hi]) + dot(s_b.astype(BF16), vb[lo:rows])
 
-    for i in range(CH):
-        relay(i)
     for i in range(n_sub):
         block_scores(i)
+    pl.when(lower)(b_pass)
+    pl.when(upper)(f_pass)
 
     q = qb[...].astype(F32) * scale
     q_f = (q * jnp.exp(cum_f[...])).astype(BF16)
@@ -462,14 +509,9 @@
     n_ctx = context.shape[1]
     dk, dv = w_key.shape[1], w_value.shape[1]
     depth = w_key.shape[0]
-    zero = jnp.zeros_like(decay_up[0])
-    up = jnp.concatenate(
-        [
-            jnp.concatenate([decay_up[0], zero], axis=1),
-            jnp.concatenate([zero, decay_up[1]], axis=1),
-        ],
-        axis=0,
-    )
+    vectors = lax.optimization_barrier(
+        jnp.concatenate([gain_pre, gain_post, cond_ctx, head_gain])
+    )[None]
     mod_in, mod_cols = w_shift.shape
     vm = pl.BlockSpec(memory_space=pltpu.VMEM)
     hbm = pl.BlockSpec(memory_space=pl.ANY)
@@ -498,19 +540,18 @@
     ]
     out = pl.pallas_call(
         functools.partial(kernel, n_sp, n_tp, n_dp),
-        out_shape=jax.ShapeDtypeStruct((rows_own, width), BF16),
-        in_specs=[vm, vm, vm, vm, hbm, hbm, hbm, vm, vm, hbm, hbm, hbm, hbm, vm, vm, vm, vm, hbm],
+        out_shape=jax.ShapeDtypeStruct((1, rows_own, width), BF16),
+        in_specs=[vm, vm, vm, vm, hbm, hbm, hbm, hbm, hbm, hbm, hbm, vm, vm, vm, hbm],
         out_specs=vm,
         scratch_shapes=scratch,
         compiler_params=pltpu.CompilerParams(
             collective_id=0, has_side_effects=True, vmem_limit_bytes=60 * 1024 * 1024
         ),
     )(
-        latents[0], cond, cond_ctx[None], context[0], w_shift, w_scale, w_gate,
-        gain_pre[None], gain_post[None], w_query, w_key, w_value, w_outgate, w_down, up,
-        decay_bias.reshape(1, -1), head_gain[None], w_out,
+        latents, cond, vectors, context, w_shift, w_scale, w_gate, w_query, w_key, w_value,
+        w_outgate, w_down.T, decay_up, decay_bias, w_out,
     )
-    return out[None]
+    return out
 
 
 def solution(mesh):

time: 237 us -> 95.7 us (0.40)
  Pallas kernels: 225 us -> 92.2 us
  local copies, waits for them, and re-layouts: 11.3 us -> 2.51 us
    pallas_call x1, Pallas kernels: 225 us -> 92.2 us  [body(): pl.pallas_call(functools.partial(kernel, n_sp, n_tp, n_dp), out_shape=jax...]
    broadcast_in_dim x4 -> x1, local copies, waits for them, and re-layouts: 5.15 us -> 0.64 us  [body(): lax.optimization_barrier(jnp.concatenate([gain_pre, gain_post, cond_ctx,...]
    unnamed x3 -> x1, local copies, waits for them, and re-layouts: 5.41 us -> 1.87 us
where the time goes in v2:
time: 95.7 us; the launch traced here: 95.5 us
  Pallas kernels  92.2 us (96%)
  local copies, waits for them, and re-layouts  2.51 us (3%)
    pallas_call x1, Pallas kernels, body(): pl.pallas_call(functools.partial(kernel, n_sp, n_tp, n_dp), out_shape=jax...  92.2 us

profile of v2, /device:TPU:0, one launch (start us, length us, event | category | flops | bytes accessed | tf_op | source)
XLA Modules:
  0.0 95.5 jit_solution(5677033657059446974)
XLA Ops:
  0.0 0.8 pad_maximum_fusion
  0.8 0.6 broadcast_in_dim.3.vec_ref
  1.4 92.2 %shard_map.172 = bf16[1,64,4096]{2,1,0:T(8,128)(2,1)} custom-call(bf16[1,64,4096]{2,1,0:T(8,128)(2,1)} %lat3.1, bf16[1,1024]{1,0:T(2,128)(2,1)} %cond_ref.1, bf16[1,9728]{1,0:T(2,128)(2,1)} %broadcast_in_dim.3.vec_ref, bf16[1,256,4096]{2,1,0:T(8,128)(2,1)} %ctx3.1, bf16[1024,1024]{1,0:T(8,128)(2,1)} %wsh_hbm.1, bf16[1024,1024]{1,0:T(8,128)(2,1)} %wsc_hbm.1, ...), custom_call_target="tpu_custom_call" | custom-call | tf_op jit(solution)/shard_map/pallas_call | solution.py:541
  93.6 1.9 %copy.20 = bf16[1,64,4096]{2,1,0:T(8,128)(2,1)} copy(bf16[1,64,4096]{2,1,0:T(8,128)(2,1)} %shard_map.172) | data formatting | bytes 1048576

commit v3 on v2

--- a/solution.py
+++ b/solution.py
@@ -11,7 +11,7 @@
 EPS = 1e-06
 TAU = 16.0
 SUB = 64
-CH = 4
+CH = 8
 MESH = pl.DeviceIdType.MESH
 F32 = jnp.float32
 BF16 = jnp.bfloat16

time: 95.7 us -> 94.6 us (0.989)
  Pallas kernels: 92.2 us -> 91.1 us
    pallas_call x1, Pallas kernels: 92.2 us -> 91.1 us  [body(): pl.pallas_call(functools.partial(kernel, n_sp, n_tp, n_dp), out_shape=jax...]
where the time goes in v3:
time: 94.6 us; the launch traced here: 94.4 us
  Pallas kernels  91.1 us (96%)
  local copies, waits for them, and re-layouts  2.51 us (3%)
    pallas_call x1, Pallas kernels, body(): pl.pallas_call(functools.partial(kernel, n_sp, n_tp, n_dp), out_shape=jax...  91.1 us

profile of v3, /device:TPU:0, one launch (start us, length us, event | category | flops | bytes accessed | tf_op | source)
XLA Modules:
  0.0 94.4 jit_solution(8752398320176345250)
XLA Ops:
  0.0 0.8 pad_maximum_fusion
  0.8 0.6 broadcast_in_dim.3.vec_ref
  1.4 91.1 %shard_map.172 = bf16[1,64,4096]{2,1,0:T(8,128)(2,1)} custom-call(bf16[1,64,4096]{2,1,0:T(8,128)(2,1)} %lat3.1, bf16[1,1024]{1,0:T(2,128)(2,1)} %cond_ref.1, bf16[1,9728]{1,0:T(2,128)(2,1)} %broadcast_in_dim.3.vec_ref, bf16[1,256,4096]{2,1,0:T(8,128)(2,1)} %ctx3.1, bf16[1024,1024]{1,0:T(8,128)(2,1)} %wsh_hbm.1, bf16[1024,1024]{1,0:T(8,128)(2,1)} %wsc_hbm.1, ...), custom_call_target="tpu_custom_call" | custom-call | tf_op jit(solution)/shard_map/pallas_call | solution.py:541
  92.5 1.9 %copy.20 = bf16[1,64,4096]{2,1,0:T(8,128)(2,1)} copy(bf16[1,64,4096]{2,1,0:T(8,128)(2,1)} %shard_map.172) | data formatting | bytes 1048576
